TPU v7x, 32 devices: a whole 2x2x4 slice. The times are simulated.
32 devices in a mesh: kv: 8 (over z, y), tp: 4 (over x, core).
Axes of the slice: x: 2, y: 2, z: 4, core: 2. Of those that a mesh axis runs over, the one named last changes fastest.
Arguments:
- queries: bfloat16 [1024, 1024], P('kv', 'tp'), may hold values from -6 to 6
- keys: bfloat16 [1024, 512], P('kv', 'tp'), may hold values from -6 to 6
- values: bfloat16 [1024, 512], P('kv', 'tp'), may hold values from -6 to 6
- hidden: bfloat16 [1024, 2048], P('kv'), may hold values from -6 to 6
- log_sums: float32 [2, 1024, 16], P(None, 'kv', 'tp'), may hold values from -1 to 12
- gates: float32 [2, 1024, 16], P(None, 'kv', 'tp'), may hold values from 0.1 to 0.9
- branch_out: bfloat16 [2, 1024, 1024], P(None, 'kv', 'tp'), may hold values from -6 to 6
- cotangent: bfloat16 [1024, 1024], P('kv', 'tp'), may hold values from -6 to 6
- chosen: int32 [8, 8, 48], P(None, 'tp'), may hold values from -1 to 31, as said below
Outputs:
- grad_queries: float32 [1024, 1024], P('kv', 'tp')
- grad_keys: float32 [1024, 512], P('kv', 'tp')
- grad_values: float32 [1024, 512], P('kv', 'tp')
- grad_weight: float32 [2048, 1024], P('kv', 'tp')
Inputs may be any that keep to these rules, and one draw needn't show every extreme that they name: `chosen`: each list holds global block numbers or -1. All live entries of one list name blocks of distinct owners, owner = entry // 4, none later than the list's range; list d holds min(48, d + 1) live entries, and they come first.
All inputs are finite; a program needn't handle non-finite values.
Results may differ from a plain program's by a relative error of at most 0.0055.
Values may be sent and summed in bfloat16 or wider, within the bound.
A program may use at most 64 MiB of HBM per device.

v0:
```python
import jax
import jax.numpy as jnp
from jax import lax
from jax.sharding import PartitionSpec as P

DH = 64
BLK = 32
TOPN = 12
SUB = 4
CMP = 32


def branch_grads(query_rows, key_rows, value_rows, seen, log_rows, delta_rows, cot_rows, scale):
    wide = jnp.float32
    scores = jnp.einsum("tgre,gme->grtm", query_rows, key_rows, preferred_element_type=wide) * scale
    log_here = jnp.transpose(log_rows, (1, 2, 0))[..., None]
    delta_here = jnp.transpose(delta_rows, (1, 2, 0))[..., None]
    probs = jnp.where(seen[:, None], jnp.exp(scores - log_here), 0.0)
    probs_low = probs.astype(jnp.bfloat16)
    value_grad = jnp.einsum("grtm,tgre->gme", probs_low, cot_rows, preferred_element_type=wide)
    prob_grad = jnp.einsum("tgre,gme->grtm", cot_rows, value_rows, preferred_element_type=wide)
    score_low = (probs * (prob_grad - delta_here)).astype(jnp.bfloat16)
    query_grad = (
        jnp.einsum("grtm,gme->tgre", score_low, key_rows, preferred_element_type=wide) * scale
    )
    key_grad = (
        jnp.einsum("grtm,tgre->gme", score_low, query_rows, preferred_element_type=wide) * scale
    )
    return (query_grad, key_grad, value_grad)


def shards(queries, keys, values, hidden, log_sums, gates, branch_out, cotangent, chosen):
    wide = jnp.float32
    rows_here = queries.shape[0]
    heads = queries.shape[1] // DH
    groups = keys.shape[1] // DH
    group_heads = heads // groups
    per_block = rows_here // BLK
    per_summary = rows_here // CMP
    blocks_all = chosen.shape[0]
    nsel = chosen.shape[2]
    qrows = rows_here // SUB
    scale = DH ** (-0.5)
    grads_each = jax.vmap(branch_grads, in_axes=(0, 0, 0, 0, 0, 0, 0, None))
    place = lax.axis_index("kv")
    position = place * rows_here + jnp.arange(rows_here, dtype=jnp.int32)
    gated = gates[..., None] * cotangent.reshape(rows_here, heads, DH).astype(wide)[None]
    delta_all = jnp.sum(gated * branch_out.reshape(2, rows_here, heads, DH).astype(wide), -1)
    delta_all = delta_all.reshape(2, rows_here, groups, group_heads)
    gated_low = gated.astype(jnp.bfloat16).reshape(2, rows_here, groups, group_heads, DH)
    log_all = log_sums.reshape(2, rows_here, groups, group_heads)
    query_all = queries.reshape(rows_here, groups, group_heads, DH)
    pairs = jnp.concatenate(
        [keys.reshape(rows_here, groups, DH), values.reshape(rows_here, groups, DH)], -1
    )
    means = jnp.mean(pairs.reshape(per_summary, CMP, groups, 2 * DH).astype(wide), 1).astype(
        jnp.bfloat16
    )
    summaries = lax.all_gather(means, "kv", axis=0, tiled=True)
    summary_count = summaries.shape[0]
    sum_keys = jnp.transpose(summaries[..., :DH], (1, 0, 2))
    sum_values = jnp.transpose(summaries[..., DH:], (1, 0, 2))
    summary_end = jnp.arange(summary_count, dtype=jnp.int32) * CMP + CMP - 1
    summary_seen = (summary_end[None, :] <= position[:, None])[None]
    query_sum, key_sum, value_sum = branch_grads(
        query_all, sum_keys, sum_values, summary_seen, log_all[0], delta_all[0], gated_low[0], scale
    )
    summary_term = jnp.transpose(jnp.concatenate([key_sum, value_sum], -1), (1, 0, 2))
    listing = lax.dynamic_index_in_dim(chosen, place, 0, keepdims=False)
    live = listing >= 0
    safe = jnp.maximum(listing, 0)
    owner = safe // per_block
    group_index = jnp.arange(groups, dtype=jnp.int32)
    hits = (chosen >= 0) & (chosen // per_block == place)
    wanted = jnp.sum(jnp.where(hits, chosen % per_block, 0), -1)
    asked = jnp.any(hits, -1)
    row_target = safe[..., None] * BLK + jnp.arange(BLK, dtype=jnp.int32)
    pair_blocks = pairs.reshape(per_block, BLK, groups, 2 * DH)
    outbound = pair_blocks[wanted, :, group_index[None, :], :]
    arrived = lax.all_to_all(outbound, "kv", split_axis=0, concat_axis=0, tiled=True)
    picked = arrived[owner, group_index[:, None]]

    def by_sub(array):
        rest = array.shape[3:]
        moved = array.reshape((groups, SUB, TOPN * BLK) + rest)
        return jnp.swapaxes(moved, 0, 1)

    picked_sub = by_sub(picked)
    picked_keys = picked_sub[..., :DH]
    picked_values = picked_sub[..., DH:]
    live_rows = by_sub(jnp.broadcast_to(live[..., None], (groups, nsel, BLK)))
    key_position = by_sub(row_target)
    sub_position = position.reshape(SUB, qrows)
    block_seen = live_rows[:, :, None, :] & (
        key_position[:, :, None, :] <= sub_position[:, None, :, None]
    )
    query_sel, key_sel, value_sel = grads_each(
        query_all.reshape(SUB, qrows, groups, group_heads, DH),
        picked_keys,
        picked_values,
        block_seen,
        log_all[1].reshape(SUB, qrows, groups, group_heads),
        delta_all[1].reshape(SUB, qrows, groups, group_heads),
        gated_low[1].reshape(SUB, qrows, groups, group_heads, DH),
        scale,
    )
    query_sel = query_sel.reshape(rows_here, groups, group_heads, DH)
    key_sel = jnp.swapaxes(key_sel, 0, 1).reshape(groups, nsel, BLK, DH)
    value_sel = jnp.swapaxes(value_sel, 0, 1).reshape(groups, nsel, BLK, DH)
    slot_grads = jnp.concatenate([key_sel, value_sel], -1)
    slot_grads = slot_grads * live[..., None, None].astype(wide)
    outgoing = (
        jnp.zeros((blocks_all, groups, BLK, 2 * DH), wide)
        .at[owner, group_index[:, None]]
        .add(slot_grads)
    )
    summary_out = jnp.transpose(
        summary_term.reshape(blocks_all, per_summary, groups, 2 * DH), (0, 2, 1, 3)
    )
    both_out = jnp.concatenate([outgoing, summary_out], 2)
    both_in = lax.all_to_all(
        both_out.astype(jnp.bfloat16), "kv", split_axis=0, concat_axis=0, tiled=True
    ).astype(both_out.dtype)
    incoming = both_in[:, :, :BLK]
    summary_mine = jnp.transpose(jnp.sum(both_in[:, :, BLK:], 0), (1, 0, 2))
    selector = (
        (wanted[..., None] == jnp.arange(per_block, dtype=jnp.int32)) & asked[..., None]
    ).astype(wide)
    block_sums = jnp.einsum("rgb,rgkc->bkgc", selector, incoming, precision=lax.Precision.HIGHEST)
    pair_grads = (
        block_sums.reshape(rows_here, groups, 2 * DH) + jnp.repeat(summary_mine, CMP, axis=0) / CMP
    )
    grad_queries = (query_sum + query_sel).reshape(rows_here, heads * DH)
    query_low = grad_queries.astype(jnp.bfloat16)
    grad_weight = lax.psum_scatter(
        lax.dot_general(
            hidden, query_low, (((0,), (0,)), ((), ())), preferred_element_type=jnp.float32
        ),
        "kv",
        scatter_dimension=0,
        tiled=True,
    )
    grad_keys = pair_grads[..., :DH].reshape(rows_here, groups * DH)
    grad_values = pair_grads[..., DH:].reshape(rows_here, groups * DH)
    return (grad_queries, grad_keys, grad_values, grad_weight)


def solution(mesh):
    return jax.shard_map(
        shards,
        mesh=mesh,
        in_specs=(
            P("kv", "tp"),
            P("kv", "tp"),
            P("kv", "tp"),
            P("kv", None),
            P(None, "kv", "tp"),
            P(None, "kv", "tp"),
            P(None, "kv", "tp"),
            P("kv", "tp"),
            P(None, "tp", None),
        ),
        out_specs=(P("kv", "tp"), P("kv", "tp"), P("kv", "tp"), P("kv", "tp")),
        check_vma=False,
    )
```

profile of v0, /device:TPU:0, one launch (start us, length us, event | category | flops | bytes accessed | tf_op | source)
XLA Modules:
  0.0 136.0 jit_solution(15902463175480948571)
XLA Ops:
  7.2 1.0 fusion.44
  8.2 0.9 fusion.33
  9.1 0.1 copy.157
  9.2 0.1 copy.158
  9.3 0.1 reshape.249
  9.4 0.8 concatenate.26
  10.3 0.8 concatenate.27
  11.1 0.1 convert_reduce_fusion
  11.3 1.3 gather_fusion
  12.5 7.3 %all-to-all-start = ((bf16[8,2,32,128]{3,2,1,0:T(8,128)(2,1)}), bf16[8,2,32,128]{3,2,1,0:T(8,128)(2,1)S(1)}, u32[]{:S(2)}, u32[]{:S(2)}) async-start(bf16[8,2,32,128]{3,2,1,0:T(8,128)(2,1)} %bitcast.20), calls=%async_computation | async-start | bytes 262144 | tf_op jit(solution)/shard_map/all_to_all | solution.py:80
  19.9 0.7 multiply_bitcast_fusion.1
  20.6 0.7 fusion.45
  21.3 0.7 or_select_fusion
  22.0 1.0 copy.153
  22.9 1.0 reshape_reshape.3
  23.9 0.1 reshape.255
  24.0 0.1 add.117
  24.1 0.1 broadcast_in_dim.36
  24.2 0.1 reshape.239
  24.4 0.1 add.115
  24.5 26.6 %all_gather.3 = bf16[32,2,128]{2,1,0:T(2,128)(2,1)S(1)} all-gather(bf16[4,2,128]{2,1,0:T(2,128)(2,1)S(1)} %multiply_convert_fusion.1), channel_id=1, replica_groups=mesh['kv'=8,'tp'=4] {'kv'}, dimensions={0}, use_global_device_ids=true | all-gather | bytes 18432 | tf_op jit(solution)/shard_map/all_gather | solution.py:59
  51.1 0.1 fusion.48
  51.2 0.1 copy.155
  51.4 0.1 copy.156
  51.7 0.1 compare_and_fusion
  51.8 0.1 fusion.18
  52.0 0.1 reshape_squeeze.9
  52.1 0.1 reshape_squeeze.11
  52.2 0.1 copy.164
  52.3 0.1 fusion.19
  52.4 1.2 gather_fusion.1
  53.6 0.4 copy.159
  54.0 0.3 fusion.5
  54.3 0.3 fusion.8
  54.6 0.3 fusion.9
  54.9 0.3 copy-done.1
  55.2 0.1 copy.168
  55.3 0.2 fusion.12
  55.5 1.8 %convolution_bitcast_fusion = f32[2048,256]{0,1:T(8,128)} fusion(bf16[128,2048]{1,0:T(8,128)(2,1)S(1)} %copy-done, f32[128,256]{0,1:T(8,128)S(1)} %bitcast.188), kind=kOutput, calls=%fused_computation.3 | convolution fusion | flops 134250496 | bytes 2752512 | tf_op jit(solution)/shard_map/dot_general | solution.py:136
  57.3 0.1 reshape.261
  57.4 0.1 fusion.21
  57.5 0.1 fusion.22
  57.7 0.1 pad_maximum_fusion.2
  57.8 0.4 copy-done.3
  58.2 0.3 fusion.7
  58.5 0.5 copy.170
  59.0 1.4 %convolution_bitcast_fusion.1 = f32[2,4,384,64]{2,3,0,1:T(8,128)S(1)} fusion(f32[4,2,2,32,384]{4,3,2,1,0:T(8,128)} %copy-done.1, bf16[4,32,2,2,64]{4,1,0,3,2:T(8,128)(2,1)S(1)} %bitcast.187), kind=kOutput, calls=%fused_computation.5 | convolution fusion | flops 25362432 | bytes 1638400 | tf_op jit(solution)/shard_map/vmap(grtm,tgre->gme)/dot_general | solution.py:20
  60.4 1.6 %copy.172 = f32[2,4,384,64]{3,2,1,0:T(8,128)} copy(f32[2,4,384,64]{2,3,0,1:T(8,128)S(1)} %convolution_bitcast_fusion.1) | data formatting | bytes 1572864 | tf_op jit(solution)/shard_map/transpose | solution.py:109
  62.1 3.2 %maximum_multiply_fusion = f32[2,48,32,128]{3,2,1,0:T(8,128)} fusion(f32[2,48,32,64]{3,2,1,0:T(8,128)} %bitcast.180, f32[2,48,32,64]{3,2,1,0:T(8,128)S(1)} %bitcast.178, f32[2,48]{1,0:T(2,128)S(1)} %get-tuple-element.30), kind=kLoop, calls=%fused_computation.4 | loop fusion | flops 786432 | bytes 3146112 | tf_op jit(solution)/shard_map/mul | solution.py:111
  65.3 9.7 %scatter_fusion = f32[8,2,32,128]{3,2,1,0:T(8,128)S(1)} fusion(f32[8,2,32,128]{3,2,1,0:T(8,128)S(1)} %broadcast_in_dim.39, s32[96]{0:T(128)S(1)} %reshape.261, f32[96,32,128]{2,1,0:T(8,128)} %bitcast.179), kind=kCustom, calls=%fused_computation.2 | custom fusion | flops 393216 | bytes 4719360 | tf_op jit(solution)/shard_map/scatter-add | solution.py:115
  75.1 0.8 copy.174
  75.9 3.9 %all-to-all-start.1 = ((bf16[8,2,36,128]{3,1,2,0:T(2,128)(2,1)}), bf16[8,2,36,128]{3,1,2,0:T(2,128)(2,1)S(1)}, u32[]{:S(2)}, u32[]{:S(2)}) async-start(bf16[8,2,36,128]{3,1,2,0:T(2,128)(2,1)} %copy.174), calls=%async_computation.1 | async-start | bytes 294912 | tf_op jit(solution)/shard_map/all_to_all | solution.py:121
  79.8 0.1 copy.177
  79.9 0.8 copy.182
  80.6 8.5 %all-to-all-done.1 = bf16[8,2,36,128]{3,1,2,0:T(2,128)(2,1)S(1)} async-done(((bf16[8,2,36,128]{3,1,2,0:T(2,128)(2,1)}), bf16[8,2,36,128]{3,1,2,0:T(2,128)(2,1)S(1)}, u32[]{:S(2)}, u32[]{:S(2)}) %all-to-all-start.1) | async-done | bytes 147488 | tf_op jit(solution)/shard_map/all_to_all | solution.py:121
  89.2 0.1 slice.80
  89.3 0.3 fusion.10
  89.6 0.1 fusion.46
  89.7 0.1 copy.181
  89.8 0.7 copy.184
  90.5 0.1 copy.180
  90.6 0.7 copy.183
  91.3 36.1 %reduce-scatter.2.cloned.1.call-done = f32[256,256]{0,1:T(8,128)} async-done(((f32[2048,256]{0,1:T(8,128)}), f32[256,256]{0,1:T(8,128)}) %reduce-scatter.2.cloned.1.call-update) | async-done | bytes 262160 | tf_op jit(solution)/shard_map/reduce_scatter | solution.py:135
  127.4 1.8 %copy.185 = f32[256,256]{1,0:T(8,128)} copy(f32[256,256]{0,1:T(8,128)} %reduce-scatter.2.cloned.1.call-done) | data formatting | bytes 524288
  (47 shorter events, 0.6 us)
Async XLA Ops:
  7.2 48.4 %copy-start = (bf16[128,2048]{1,0:T(8,128)(2,1)S(1)}, bf16[128,2048]{1,0:T(8,128)(2,1)}, u32[]{:S(2)}) copy-start(bf16[128,2048]{1,0:T(8,128)(2,1)} %param.12) | copy-start | bytes 1572868
  7.2 16.8 %copy-start.7 = (f32[2,128,4]{1,2,0:T(4,128)S(1)}, f32[2,128,4]{1,2,0:T(4,128)}, u32[]{:S(2)}) copy-start(f32[2,128,4]{1,2,0:T(4,128)} %param.13) | copy-start | bytes 12292
  7.2 44.0 %copy-start.5 = (bf16[128,256]{1,0:T(8,128)(2,1)S(1)}, bf16[128,256]{1,0:T(8,128)(2,1)}, u32[]{:S(2)}) copy-start(bf16[128,256]{1,0:T(8,128)(2,1)} %param.16) | copy-start | bytes 196612
  7.2 44.2 %copy-start.4 = (bf16[2,128,256]{2,1,0:T(8,128)(2,1)S(1)}, bf16[2,128,256]{2,1,0:T(8,128)(2,1)}, u32[]{:S(2)}) copy-start(bf16[2,128,256]{2,1,0:T(8,128)(2,1)} %param.15) | copy-start | bytes 393220
  7.2 44.3 %copy-start.6 = (f32[2,128,4]{1,2,0:T(4,128)S(1)}, f32[2,128,4]{1,2,0:T(4,128)}, u32[]{:S(2)}) copy-start(f32[2,128,4]{1,2,0:T(4,128)} %param.14) | copy-start | bytes 12292
  12.5 39.9 %all-to-all-start = ((bf16[8,2,32,128]{3,2,1,0:T(8,128)(2,1)}), bf16[8,2,32,128]{3,2,1,0:T(8,128)(2,1)S(1)}, u32[]{:S(2)}, u32[]{:S(2)}) async-start(bf16[8,2,32,128]{3,2,1,0:T(8,128)(2,1)} %bitcast.20), calls=%async_computation | async-start | bytes 262144 | tf_op jit(solution)/shard_map/all_to_all | solution.py:80
  19.8 107.6 %reduce-scatter.2.cloned.1.call-start = ((), (), s32[]{:S(2)}) async-start(), calls=%async_computation.3 | async-start | bytes 2359296 | tf_op jit(solution)/shard_map/reduce_scatter | solution.py:135
  23.9 30.1 %copy-start.2 = (bf16[4,32,2,2,64]{4,3,2,1,0:T(2,128)(2,1)}, bf16[4,32,2,2,64]{4,3,2,1,0:T(2,128)(2,1)S(1)}, u32[]{:S(2)}) copy-start(bf16[4,32,2,2,64]{4,3,2,1,0:T(2,128)(2,1)S(1)} %reshape_reshape.3) | copy-start | bytes 196612
  54.3 0.9 copy-start.1
  57.3 0.9 copy-start.3
  75.9 13.3 %all-to-all-start.1 = ((bf16[8,2,36,128]{3,1,2,0:T(2,128)(2,1)}), bf16[8,2,36,128]{3,1,2,0:T(2,128)(2,1)S(1)}, u32[]{:S(2)}, u32[]{:S(2)}) async-start(bf16[8,2,36,128]{3,1,2,0:T(2,128)(2,1)} %copy.174), calls=%async_computation.1 | async-start | bytes 294912 | tf_op jit(solution)/shard_map/all_to_all | solution.py:121
Sparse Core Ops, SparseCore 0:
  57.4 69.8 reduce-scatter.1
where the time goes:
time: 137 us; the launch traced here: 136 us
  waiting for transfers between devices  44.6 us (33%)
  blocking collectives  26.6 us (19%)
  other arithmetic  17.5 us (13%)
  local copies, waits for them, and re-layouts  16.2 us (12%)
  between operations  14.5 us (11%)
  starting transfers between devices  11.3 us (8%)
  matrix products  5.35 us (4%)
    reduce_scatter x1, waiting for transfers between devices, shards(): lax.psum_scatter(lax.dot_general(hidden, query_low, (((0,), (0,)), ((), (...  36.1 us
    all_gather x1, blocking collectives, shards(): summaries = lax.all_gather(means, 'kv', axis=0, tiled=True)  26.6 us
    scatter-add x1, other arithmetic, shards(): outgoing = jnp.zeros((blocks_all, groups, BLK, 2 * DH), wide).at[owner, g...  9.74 us
    all_to_all x1, waiting for transfers between devices, shards(): lax.all_to_all(both_out.astype(jnp.bfloat16), 'kv', split_axis=0, concat_...  8.53 us
    all_to_all x1, starting transfers between devices, shards(): lax.all_to_all(outbound, 'kv', split_axis=0, concat_axis=0, tiled=True)  7.31 us
    unnamed x23, local copies, waits for them, and re-layouts  5.95 us
    all_to_all x1, starting transfers between devices, shards(): lax.all_to_all(both_out.astype(jnp.bfloat16), 'kv', split_axis=0, concat_...  3.92 us
    mul x1, other arithmetic, shards(): slot_grads = slot_grads * live[..., None, None].astype(wide)  3.19 us
  transfers between devices with their start and end apart: 3, of which 2 were waited for; matrix products, arithmetic and copies ran while one was open for 20% of the time, Pallas kernels for 0%

commit v1 on v0

--- a/solution.py
+++ b/solution.py
@@ -56,7 +56,12 @@
     means = jnp.mean(pairs.reshape(per_summary, CMP, groups, 2 * DH).astype(wide), 1).astype(
         jnp.bfloat16
     )
-    summaries = lax.all_gather(means, "kv", axis=0, tiled=True)
+    ring = [means]
+    for hop in range(7):
+        ring.append(lax.ppermute(ring[-1], "kv", [(dev, (dev + 1) % 8) for dev in range(8)]))
+    summaries = jnp.roll(
+        jnp.concatenate(ring[::-1], axis=0), (lax.axis_index("kv") + 1) * ring[0].shape[0], axis=0
+    )
     summary_count = summaries.shape[0]
     sum_keys = jnp.transpose(summaries[..., :DH], (1, 0, 2))
     sum_values = jnp.transpose(summaries[..., DH:], (1, 0, 2))

time: 137 us -> 144 us (1.051)
  waiting for transfers between devices: 44.6 us -> 77.1 us
  blocking collectives: 26.6 us -> 0 us
  starting transfers between devices: 11.3 us -> 13.4 us
    ppermute x0 -> x7, waiting for transfers between devices: none -> 34.2 us  [shards(): lax.ppermute(ring[-1], 'kv', [(dev, (dev + 1) % 8) for dev in range(8)])]
    all_gather x1 -> x0, blocking collectives: 26.6 us -> none  [shards(): summaries = lax.all_gather(means, 'kv', axis=0, tiled=True)]
    ppermute x0 -> x7, starting transfers between devices: none -> 5.09 us  [shards(): lax.ppermute(ring[-1], 'kv', [(dev, (dev + 1) % 8) for dev in range(8)])]
    all_to_all x1, starting transfers between devices: 7.31 us -> 4.88 us  [shards(): lax.all_to_all(outbound, 'kv', split_axis=0, concat_axis=0, tiled=True)]
    unnamed x23 -> x25, local copies, waits for them, and re-layouts: 5.95 us -> 5.52 us
  transfers between devices with their start and end apart: 3 -> 10, of which waited for: 2 -> 8; matrix products, arithmetic and copies ran while one was open for 20% -> 21% of each run, Pallas kernels for 0% -> 0%
where the time goes in v1:
time: 144 us
  waiting for transfers between devices  77.1 us (54%)
  other arithmetic  17.4 us (12%)
  local copies, waits for them, and re-layouts  15.7 us (11%)
  between operations  14.5 us (10%)
  starting transfers between devices  13.4 us (9%)
  matrix products  5.45 us (4%)
    reduce_scatter x1, waiting for transfers between devices, shards(): lax.psum_scatter(lax.dot_general(hidden, query_low, (((0,), (0,)), ((), (...  35.4 us
    ppermute x7, waiting for transfers between devices, shards(): lax.ppermute(ring[-1], 'kv', [(dev, (dev + 1) % 8) for dev in range(8)])  34.2 us
    scatter-add x1, other arithmetic, shards(): outgoing = jnp.zeros((blocks_all, groups, BLK, 2 * DH), wide).at[owner, g...  9.74 us
    all_to_all x1, waiting for transfers between devices, shards(): lax.all_to_all(both_out.astype(jnp.bfloat16), 'kv', split_axis=0, concat_...  7.43 us
    unnamed x25, local copies, waits for them, and re-layouts  5.52 us
    ppermute x7, starting transfers between devices, shards(): lax.ppermute(ring[-1], 'kv', [(dev, (dev + 1) % 8) for dev in range(8)])  5.09 us
    all_to_all x1, starting transfers between devices, shards(): lax.all_to_all(outbound, 'kv', split_axis=0, concat_axis=0, tiled=True)  4.88 us
    all_to_all x1, starting transfers between devices, shards(): lax.all_to_all(both_out.astype(jnp.bfloat16), 'kv', split_axis=0, concat_...  3.38 us
  transfers between devices with their start and end apart: 10, of which 8 were waited for; matrix products, arithmetic and copies ran while one was open for 21% of the time, Pallas kernels for 0%

profile of v1, /device:TPU:0, one launch (start us, length us, event | category | flops | bytes accessed | tf_op | source)
XLA Modules:
  0.0 143.6 jit_solution(10500187953345225336)
XLA Ops:
  7.2 0.9 concatenate.32
  8.2 0.8 concatenate.33
  9.0 0.1 convert_reduce_fusion
  9.1 3.0 %collective-permute-start = (bf16[4,2,128]{2,0,1:T(4,128)(2,1)S(1)}, bf16[4,2,128]{2,0,1:T(4,128)(2,1)S(1)}, u32[]{:S(2)}, u32[]{:S(2)}) collective-permute-start(bf16[4,2,128]{2,0,1:T(4,128)(2,1)S(1)} %fusion.34), channel_id=1, source_target_pairs={{0,4},{4,8},{8,12},{12,16},{16,20},{20,24},{24,28},{28,0},{1,5},{5... | collective-permute-start | bytes 6152 | tf_op jit(solution)/shard_map/ppermute | solution.py:61
  12.2 0.9 fusion.48
  13.1 0.9 fusion.33
  14.1 0.1 copy.155
  14.3 1.3 gather_fusion
  15.6 4.9 %all-to-all-start = ((bf16[8,2,32,128]{3,2,1,0:T(8,128)(2,1)}), bf16[8,2,32,128]{3,2,1,0:T(8,128)(2,1)S(1)}, u32[]{:S(2)}, u32[]{:S(2)}) async-start(bf16[8,2,32,128]{3,2,1,0:T(8,128)(2,1)} %bitcast.20), calls=%async_computation | async-start | bytes 262144 | tf_op jit(solution)/shard_map/all_to_all | solution.py:85
  20.5 0.7 multiply_bitcast_fusion.1
  21.2 0.7 fusion.49
  22.0 0.1 reshape.239
  22.2 0.1 add.131
  22.3 1.0 copy.152
  23.3 0.1 copy.153
  23.5 0.1 compare_and_fusion
  23.7 2.0 %collective-permute-start.1 = (bf16[4,2,128]{2,0,1:T(4,128)(2,1)S(1)}, bf16[4,2,128]{2,0,1:T(4,128)(2,1)S(1)}, u32[]{:S(2)}, u32[]{:S(2)}) collective-permute-start(bf16[4,2,128]{2,0,1:T(4,128)(2,1)S(1)} %collective-permute-done), channel_id=1, source_target_pairs={{0,4},{4,8},{8,12},{12,16},{16,20},{20,24},{24,28},{28,0},{1,5},{5... | collective-permute-start | bytes 6152 | tf_op jit(solution)/shard_map/ppermute | solution.py:61
  25.7 4.3 %collective-permute-done.1 = bf16[4,2,128]{2,0,1:T(4,128)(2,1)S(1)} collective-permute-done((bf16[4,2,128]{2,0,1:T(4,128)(2,1)S(1)}, bf16[4,2,128]{2,0,1:T(4,128)(2,1)S(1)}, u32[]{:S(2)}, u32[]{:S(2)}) %collective-permute-start.1) | collective-permute-done | bytes 2080 | tf_op jit(solution)/shard_map/ppermute | solution.py:61
  30.1 6.3 %collective-permute-done.2 = bf16[4,2,128]{2,0,1:T(4,128)(2,1)S(1)} collective-permute-done((bf16[4,2,128]{2,0,1:T(4,128)(2,1)S(1)}, bf16[4,2,128]{2,0,1:T(4,128)(2,1)S(1)}, u32[]{:S(2)}, u32[]{:S(2)}) %collective-permute-start.2) | collective-permute-done | bytes 2080 | tf_op jit(solution)/shard_map/ppermute | solution.py:61
  36.3 6.3 %collective-permute-done.3 = bf16[4,2,128]{2,0,1:T(4,128)(2,1)S(1)} collective-permute-done((bf16[4,2,128]{2,0,1:T(4,128)(2,1)S(1)}, bf16[4,2,128]{2,0,1:T(4,128)(2,1)S(1)}, u32[]{:S(2)}, u32[]{:S(2)}) %collective-permute-start.3) | collective-permute-done | bytes 2080 | tf_op jit(solution)/shard_map/ppermute | solution.py:61
  42.7 6.2 %collective-permute-done.4 = bf16[4,2,128]{2,0,1:T(4,128)(2,1)S(1)} collective-permute-done((bf16[4,2,128]{2,0,1:T(4,128)(2,1)S(1)}, bf16[4,2,128]{2,0,1:T(4,128)(2,1)S(1)}, u32[]{:S(2)}, u32[]{:S(2)}) %collective-permute-start.4) | collective-permute-done | bytes 2080 | tf_op jit(solution)/shard_map/ppermute | solution.py:61
  48.9 0.7 or_select_fusion
  49.6 5.6 %collective-permute-done.5 = bf16[4,2,128]{2,0,1:T(4,128)(2,1)S(1)} collective-permute-done((bf16[4,2,128]{2,0,1:T(4,128)(2,1)S(1)}, bf16[4,2,128]{2,0,1:T(4,128)(2,1)S(1)}, u32[]{:S(2)}, u32[]{:S(2)}) %collective-permute-start.5) | collective-permute-done | bytes 2080 | tf_op jit(solution)/shard_map/ppermute | solution.py:61
  55.2 0.1 copy.151
  55.3 0.1 reshape_reshape.3
  55.6 0.1 reshape_squeeze.9
  55.7 0.1 reshape_squeeze.11
  55.8 0.1 copy.161
  55.9 5.6 %collective-permute-done.6 = bf16[4,2,128]{2,0,1:T(4,128)(2,1)S(1)} collective-permute-done((bf16[4,2,128]{2,0,1:T(4,128)(2,1)S(1)}, bf16[4,2,128]{2,0,1:T(4,128)(2,1)S(1)}, u32[]{:S(2)}, u32[]{:S(2)}) %collective-permute-start.6) | collective-permute-done | bytes 2080 | tf_op jit(solution)/shard_map/ppermute | solution.py:61
  61.5 0.2 concatenate.35
  61.7 0.1 fusion.18
  61.8 0.2 fusion.19
  62.1 1.2 gather_fusion.1
  63.2 0.4 copy.156
  63.6 0.3 fusion.5
  63.9 0.3 fusion.8
  64.2 0.3 fusion.9
  64.5 0.3 copy-done.1
  64.8 0.1 copy.165
  64.9 0.2 fusion.12
  65.2 1.8 %convolution_bitcast_fusion = f32[2048,256]{0,1:T(8,128)} fusion(bf16[128,2048]{1,0:T(8,128)(2,1)S(1)} %copy-done, f32[128,256]{0,1:T(8,128)S(1)} %bitcast.188), kind=kOutput, calls=%fused_computation.3 | convolution fusion | flops 134250496 | bytes 2752512 | tf_op jit(solution)/shard_map/dot_general | solution.py:141
  67.0 0.1 fusion.21
  67.2 0.1 fusion.22
  67.3 0.1 pad_maximum_fusion.2
  67.4 0.6 copy.208
  68.0 0.3 fusion.7
  68.3 0.5 copy.167
  68.8 1.4 %convolution_bitcast_fusion.1 = f32[2,4,384,64]{2,3,0,1:T(8,128)S(1)} fusion(f32[4,2,2,32,384]{4,3,2,1,0:T(8,128)} %copy-done.1, bf16[4,32,2,2,64]{4,1,0,3,2:T(8,128)(2,1)S(1)} %bitcast.187), kind=kOutput, calls=%fused_computation.5 | convolution fusion | flops 25362432 | bytes 1638400 | tf_op jit(solution)/shard_map/vmap(grtm,tgre->gme)/dot_general | solution.py:20
  70.3 1.6 %copy.169 = f32[2,4,384,64]{3,2,1,0:T(8,128)} copy(f32[2,4,384,64]{2,3,0,1:T(8,128)S(1)} %convolution_bitcast_fusion.1) | data formatting | bytes 1572864 | tf_op jit(solution)/shard_map/transpose | solution.py:114
  71.9 3.2 %maximum_multiply_fusion = f32[2,48,32,128]{3,2,1,0:T(8,128)} fusion(f32[2,48,32,64]{3,2,1,0:T(8,128)} %bitcast.180, f32[2,48,32,64]{3,2,1,0:T(8,128)S(1)} %bitcast.178, f32[2,48]{1,0:T(2,128)S(1)} %get-tuple-element.30), kind=kLoop, calls=%fused_computation.4 | loop fusion | flops 786432 | bytes 3146112 | tf_op jit(solution)/shard_map/mul | solution.py:116
  75.1 9.7 %scatter_fusion = f32[8,2,32,128]{3,2,1,0:T(8,128)S(1)} fusion(f32[8,2,32,128]{3,2,1,0:T(8,128)S(1)} %broadcast_in_dim.39, s32[96]{0:T(128)S(1)} %reshape.261, f32[96,32,128]{2,1,0:T(8,128)} %bitcast.179), kind=kCustom, calls=%fused_computation.2 | custom fusion | flops 393216 | bytes 4719360 | tf_op jit(solution)/shard_map/scatter-add | solution.py:120
  84.9 0.8 copy.171
  85.7 3.4 %all-to-all-start.1 = ((bf16[8,2,36,128]{3,1,2,0:T(2,128)(2,1)}), bf16[8,2,36,128]{3,1,2,0:T(2,128)(2,1)S(1)}, u32[]{:S(2)}, u32[]{:S(2)}) async-start(bf16[8,2,36,128]{3,1,2,0:T(2,128)(2,1)} %copy.171), calls=%async_computation.1 | async-start | bytes 294912 | tf_op jit(solution)/shard_map/all_to_all | solution.py:126
  89.1 0.1 copy.174
  89.2 0.8 copy.179
  89.9 7.4 %all-to-all-done.1 = bf16[8,2,36,128]{3,1,2,0:T(2,128)(2,1)S(1)} async-done(((bf16[8,2,36,128]{3,1,2,0:T(2,128)(2,1)}), bf16[8,2,36,128]{3,1,2,0:T(2,128)(2,1)S(1)}, u32[]{:S(2)}, u32[]{:S(2)}) %all-to-all-start.1) | async-done | bytes 147488 | tf_op jit(solution)/shard_map/all_to_all | solution.py:126
  97.4 0.1 slice.78
  97.5 0.3 fusion.10
  97.8 0.1 fusion.50
  97.9 0.1 copy.178
  98.0 0.7 copy.181
  98.8 0.7 copy.180
  99.5 35.4 %reduce-scatter.2.cloned.1.call-done = f32[256,256]{0,1:T(8,128)} async-done(((f32[2048,256]{0,1:T(8,128)}), f32[256,256]{0,1:T(8,128)}) %reduce-scatter.2.cloned.1.call-update) | async-done | bytes 262160 | tf_op jit(solution)/shard_map/reduce_scatter | solution.py:140
  134.9 1.8 %copy.182 = f32[256,256]{1,0:T(8,128)} copy(f32[256,256]{0,1:T(8,128)} %reduce-scatter.2.cloned.1.call-done) | data formatting | bytes 524288
  (62 shorter events, 1.1 us)
Async XLA Ops:
  7.2 58.0 %copy-start = (bf16[128,2048]{1,0:T(8,128)(2,1)S(1)}, bf16[128,2048]{1,0:T(8,128)(2,1)}, u32[]{:S(2)}) copy-start(bf16[128,2048]{1,0:T(8,128)(2,1)} %param.12) | copy-start | bytes 1572868
  7.2 16.1 %copy-start.5 = (bf16[2,128,256]{2,1,0:T(8,128)(2,1)S(1)}, bf16[2,128,256]{2,1,0:T(8,128)(2,1)}, u32[]{:S(2)}) copy-start(bf16[2,128,256]{2,1,0:T(8,128)(2,1)} %param.15) | copy-start | bytes 393220
  7.2 16.3 %copy-start.7 = (f32[2,128,4]{1,2,0:T(4,128)S(1)}, f32[2,128,4]{1,2,0:T(4,128)}, u32[]{:S(2)}) copy-start(f32[2,128,4]{1,2,0:T(4,128)} %param.14) | copy-start | bytes 12292
  7.2 16.5 %copy-start.8 = (f32[2,128,4]{1,2,0:T(4,128)S(1)}, f32[2,128,4]{1,2,0:T(4,128)}, u32[]{:S(2)}) copy-start(f32[2,128,4]{1,2,0:T(4,128)} %param.13) | copy-start | bytes 12292
  7.2 48.0 %copy-start.4 = (bf16[128,256]{1,0:T(8,128)(2,1)S(1)}, bf16[128,256]{1,0:T(8,128)(2,1)}, u32[]{:S(2)}) copy-start(bf16[128,256]{1,0:T(8,128)(2,1)} %param.9) | copy-start | bytes 196612
  9.1 14.6 %collective-permute-start = (bf16[4,2,128]{2,0,1:T(4,128)(2,1)S(1)}, bf16[4,2,128]{2,0,1:T(4,128)(2,1)S(1)}, u32[]{:S(2)}, u32[]{:S(2)}) collective-permute-start(bf16[4,2,128]{2,0,1:T(4,128)(2,1)S(1)} %fusion.34), channel_id=1, source_target_pairs={{0,4},{4,8},{8,12},{12,16},{16,20},{20,24},{24,28},{28,0},{1,5},{5... | collective-permute-start | bytes 6152 | tf_op jit(solution)/shard_map/ppermute | solution.py:61
  15.6 46.5 %all-to-all-start = ((bf16[8,2,32,128]{3,2,1,0:T(8,128)(2,1)}), bf16[8,2,32,128]{3,2,1,0:T(8,128)(2,1)S(1)}, u32[]{:S(2)}, u32[]{:S(2)}) async-start(bf16[8,2,32,128]{3,2,1,0:T(8,128)(2,1)} %bitcast.20), calls=%async_computation | async-start | bytes 262144 | tf_op jit(solution)/shard_map/all_to_all | solution.py:85
  20.4 114.5 %reduce-scatter.2.cloned.1.call-start = ((), (), s32[]{:S(2)}) async-start(), calls=%async_computation.3 | async-start | bytes 2359296 | tf_op jit(solution)/shard_map/reduce_scatter | solution.py:140
  23.7 6.3 %collective-permute-start.1 = (bf16[4,2,128]{2,0,1:T(4,128)(2,1)S(1)}, bf16[4,2,128]{2,0,1:T(4,128)(2,1)S(1)}, u32[]{:S(2)}, u32[]{:S(2)}) collective-permute-start(bf16[4,2,128]{2,0,1:T(4,128)(2,1)S(1)} %collective-permute-done), channel_id=1, source_target_pairs={{0,4},{4,8},{8,12},{12,16},{16,20},{20,24},{24,28},{28,0},{1,5},{5... | collective-permute-start | bytes 6152 | tf_op jit(solution)/shard_map/ppermute | solution.py:61
  30.1 6.3 %collective-permute-start.2 = (bf16[4,2,128]{2,0,1:T(4,128)(2,1)S(1)}, bf16[4,2,128]{2,0,1:T(4,128)(2,1)S(1)}, u32[]{:S(2)}, u32[]{:S(2)}) collective-permute-start(bf16[4,2,128]{2,0,1:T(4,128)(2,1)S(1)} %collective-permute-done.1), channel_id=1, source_target_pairs={{0,4},{4,8},{8,12},{12,16},{16,20},{20,24},{24,28},{28,0},{1,5},{5... | collective-permute-start | bytes 6152 | tf_op jit(solution)/shard_map/ppermute | solution.py:61
  36.3 6.3 %collective-permute-start.3 = (bf16[4,2,128]{2,0,1:T(4,128)(2,1)S(1)}, bf16[4,2,128]{2,0,1:T(4,128)(2,1)S(1)}, u32[]{:S(2)}, u32[]{:S(2)}) collective-permute-start(bf16[4,2,128]{2,0,1:T(4,128)(2,1)S(1)} %collective-permute-done.2), channel_id=1, source_target_pairs={{0,4},{4,8},{8,12},{12,16},{16,20},{20,24},{24,28},{28,0},{1,5},{5... | collective-permute-start | bytes 6152 | tf_op jit(solution)/shard_map/ppermute | solution.py:61
  42.6 6.3 %collective-permute-start.4 = (bf16[4,2,128]{2,0,1:T(4,128)(2,1)S(1)}, bf16[4,2,128]{2,0,1:T(4,128)(2,1)S(1)}, u32[]{:S(2)}, u32[]{:S(2)}) collective-permute-start(bf16[4,2,128]{2,0,1:T(4,128)(2,1)S(1)} %collective-permute-done.3), channel_id=1, source_target_pairs={{0,4},{4,8},{8,12},{12,16},{16,20},{20,24},{24,28},{28,0},{1,5},{5... | collective-permute-start | bytes 6152 | tf_op jit(solution)/shard_map/ppermute | solution.py:61
  48.9 6.3 %collective-permute-start.5 = (bf16[4,2,128]{2,0,1:T(4,128)(2,1)S(1)}, bf16[4,2,128]{2,0,1:T(4,128)(2,1)S(1)}, u32[]{:S(2)}, u32[]{:S(2)}) collective-permute-start(bf16[4,2,128]{2,0,1:T(4,128)(2,1)S(1)} %collective-permute-done.4), channel_id=1, source_target_pairs={{0,4},{4,8},{8,12},{12,16},{16,20},{20,24},{24,28},{28,0},{1,5},{5... | collective-permute-start | bytes 6152 | tf_op jit(solution)/shard_map/ppermute | solution.py:61
  55.2 6.3 %collective-permute-start.6 = (bf16[4,2,128]{2,0,1:T(4,128)(2,1)S(1)}, bf16[4,2,128]{2,0,1:T(4,128)(2,1)S(1)}, u32[]{:S(2)}, u32[]{:S(2)}) collective-permute-start(bf16[4,2,128]{2,0,1:T(4,128)(2,1)S(1)} %collective-permute-done.5), channel_id=1, source_target_pairs={{0,4},{4,8},{8,12},{12,16},{16,20},{20,24},{24,28},{28,0},{1,5},{5... | collective-permute-start | bytes 6152 | tf_op jit(solution)/shard_map/ppermute | solution.py:61
  55.5 8.1 %copy-start.2 = (bf16[4,32,2,2,64]{4,3,2,1,0:T(2,128)(2,1)}, bf16[4,32,2,2,64]{4,3,2,1,0:T(2,128)(2,1)S(1)}, u32[]{:S(2)}) copy-start(bf16[4,32,2,2,64]{4,3,2,1,0:T(2,128)(2,1)S(1)} %reshape_reshape.3) | copy-start | bytes 196612
  63.9 0.9 copy-start.1
  66.9 1.1 copy-start.3
  75.1 9.8 %copy-start.6 = (bf16[8,4,2,128]{3,1,2,0:T(4,128)(2,1)S(1)}, bf16[8,4,2,128]{3,1,2,0:T(4,128)(2,1)}, u32[]{:S(2)}) copy-start(bf16[8,4,2,128]{3,1,2,0:T(4,128)(2,1)} %copy.208) | copy-start | bytes 49156
  85.7 11.7 %all-to-all-start.1 = ((bf16[8,2,36,128]{3,1,2,0:T(2,128)(2,1)}), bf16[8,2,36,128]{3,1,2,0:T(2,128)(2,1)S(1)}, u32[]{:S(2)}, u32[]{:S(2)}) async-start(bf16[8,2,36,128]{3,1,2,0:T(2,128)(2,1)} %copy.171), calls=%async_computation.1 | async-start | bytes 294912 | tf_op jit(solution)/shard_map/all_to_all | solution.py:126
Sparse Core Ops, SparseCore 0:
  67.1 67.8 reduce-scatter.1
